TPU v7x, 32 devices: a whole 2x2x4 slice. The times are simulated.
32 devices in a mesh: sp: 8 (over z, y), tp: 4 (over x, core).
Axes of the slice: x: 2, y: 2, z: 4, core: 2. Of those that a mesh axis runs over, the one named last changes fastest.
Arguments:
- residual_entry_input: bfloat16 [8192, 2048], P(('sp', 'tp')), may hold values from -6 to 6
- query_matrix_rows: bfloat16 [8192, 1024], P('sp', 'tp'), may hold values from -6 to 6
- key_matrix_rows: bfloat16 [8192, 1024], P('sp', 'tp'), may hold values from -6 to 6
- value_matrix_rows: bfloat16 [8192, 2048], P('sp', 'tp'), may hold values from -6 to 6
- output_gate_logits: bfloat16 [8192, 2048], P('sp', 'tp'), may hold values from -6 to 6
- input_gate_logits: float32 [8192, 8], P('sp', 'tp'), may hold values from -6 to 6
- forget_gate_logits: float32 [8192, 8], P('sp', 'tp'), may hold values from -8 to 31
- forget_decay_offset: float32 [8192, 8], P('sp', 'tp'), may hold values from -0.7 to 0
- head_norm_gain: float32 [8, 256], P('tp'), may hold values from 0.1 to 1.9
- cell_output_weight: bfloat16 [2048, 2048], P('tp'), may hold values from -0.125 to 0.125
- feedforward_norm_gain: float32 [2048], replicated, may hold values from 0.1 to 1.9
- gate_up_weight: bfloat16 [2048, 5632], P('sp', 'tp'), may hold values from -0.125 to 0.125
- value_up_weight: bfloat16 [2048, 5632], P('sp', 'tp'), may hold values from -0.125 to 0.125
- gate_filter_taps: float32 [3, 5632], P(None, 'tp'), may hold values from -3 to 3
- value_filter_taps: float32 [3, 5632], P(None, 'tp'), may hold values from -3 to 3
- down_projection_weight: bfloat16 [5632, 2048], P('tp', 'sp'), may hold values from -0.078125 to 0.078125
Outputs:
- result: bfloat16 [8192, 2048], P(('sp', 'tp'))
All inputs are finite; a program needn't handle non-finite values.
Results may differ from a plain program's by a relative error of at most 0.025.
Values may be sent and summed in bfloat16 or wider, within the bound.
No kernel may reach another device: no remote copies, remote signals or barrier semaphores. Data moves between devices by JAX's collectives and lax.ppermute only.
A program may use at most 128 MiB of HBM per device.

v0:
```python
import jax
import jax.numpy as jnp
from jax import lax
from jax.sharding import PartitionSpec as P

BLOCK = 128
eps = 1e-06
neg_large = -1e30


def carried_in(x, axis, combine, identity):
    count, position = (lax.axis_size(axis), lax.axis_index(axis))
    everything = jax.tree.map(
        lambda part, kind: lax.all_gather(part.astype(kind), axis),
        x,
        (jnp.bfloat16, jnp.bfloat16, jnp.bfloat16, jnp.bfloat16),
    )
    start = jax.tree.map(
        lambda part, zero: jnp.broadcast_to(jnp.asarray(zero, part.dtype), part.shape), x, identity
    )

    def lap(k, before):
        reached = k < position
        new = combine(
            before, jax.tree.map(lambda part, own: part[k].astype(own.dtype), everything, x)
        )
        return jax.tree.map(lambda a, b: jnp.where(reached, a, b), new, before)

    return lax.fori_loop(0, count, lap, start)


def shifted(x, axis, by):
    count = lax.axis_size(axis)
    pairs = [(i, i + by) for i in range(count) if 0 <= i + by < count]
    return lax.ppermute(x, axis, pairs)


def gate_log_values(input_gate_logits, forget_gate_logits, forget_decay_offset):
    input_log_value = 15.0 * jnp.tanh(input_gate_logits / 15.0)
    forget_log_sigmoid = (
        jax.nn.log_sigmoid(15.0 * jnp.tanh(forget_gate_logits / 15.0)) + forget_decay_offset
    )
    return (input_log_value, forget_log_sigmoid)


def combine_states(earlier, later):
    total_one, memory_one, normer_one, running_one = earlier
    total_two, memory_two, normer_two, running_two = later
    joined = jnp.maximum(total_two + running_one, running_two)
    weight_one = jnp.exp(total_two + running_one - joined)
    weight_two = jnp.exp(running_two - joined)
    memory = weight_one[:, None, None] * memory_one + weight_two[:, None, None] * memory_two
    normer = weight_one[:, None] * normer_one + weight_two[:, None] * normer_two
    return (total_one + total_two, memory, normer, joined)


def local_step(state_carry, inputs):
    memory, normer, running = state_carry
    query_block, key_block, value_block, input_block, forget_block = inputs
    length = query_block.shape[0]
    highest = lax.Precision.HIGHEST
    query_scale = query_block.shape[2] ** (-0.5)
    causal = jnp.tril(jnp.ones((length, length), dtype=bool))[:, :, None]
    cumulative = jnp.cumsum(forget_block, axis=0)
    logits = cumulative[:, None, :] - cumulative[None, :, :] + input_block[None, :, :]
    logits = jnp.where(causal, logits, -jnp.inf)
    carried = cumulative + running[None, :]
    stable = jnp.maximum(carried, jnp.max(logits, axis=1))
    carry_weight = jnp.exp(carried - stable)
    raw = (
        jnp.einsum("thd,shd->tsh", query_block, key_block, preferred_element_type=jnp.float32)
        * query_scale
    )
    scores = raw * jnp.exp(logits - stable[:, None, :])
    scaled_query = query_block.astype(jnp.float32) * query_scale
    numerator = carry_weight[:, :, None] * jnp.einsum(
        "hvd,thd->thv", memory, scaled_query, precision=highest
    )
    numerator = numerator + jnp.einsum(
        "tsh,shv->thv", scores.astype(jnp.bfloat16), value_block, preferred_element_type=jnp.float32
    )
    denominator = carry_weight * jnp.einsum(
        "hd,thd->th", normer, scaled_query, precision=highest
    ) + jnp.sum(scores, axis=1)
    last_sum = cumulative[-1]
    weights_log = last_sum[None, :] - cumulative + input_block
    new_running = jnp.maximum(last_sum + running, jnp.max(weights_log, axis=0))
    decay_factor = jnp.exp(last_sum + running - new_running)
    weighted = (
        key_block.astype(jnp.float32) * jnp.exp(weights_log - new_running[None, :])[:, :, None]
    )
    memory = decay_factor[:, None, None] * memory + jnp.einsum(
        "shv,shd->hvd",
        value_block,
        weighted.astype(jnp.bfloat16),
        preferred_element_type=jnp.float32,
    )
    normer = decay_factor[:, None] * normer + jnp.sum(weighted, axis=0)
    return ((memory, normer, new_running), (numerator, denominator, stable))


def local(
    residual_entry_input,
    query_matrix_rows,
    key_matrix_rows,
    value_matrix_rows,
    output_gate_logits,
    input_gate_logits,
    forget_gate_logits,
    forget_decay_offset,
    head_norm_gain,
    cell_output_weight,
    feedforward_norm_gain,
    gate_up_weight,
    value_up_weight,
    gate_filter_taps,
    value_filter_taps,
    down_projection_weight,
):
    highest = lax.Precision.HIGHEST
    token_count = query_matrix_rows.shape[0]
    head_count = input_gate_logits.shape[1]
    key_width = query_matrix_rows.shape[1] // head_count
    value_width = value_matrix_rows.shape[1] // head_count
    query_scale = key_width ** (-0.5)
    queries_low = query_matrix_rows.reshape(token_count, head_count, key_width)
    keys_low = key_matrix_rows.reshape(token_count, head_count, key_width)
    values_low = value_matrix_rows.reshape(token_count, head_count, value_width)
    input_log_value, forget_log_sigmoid = gate_log_values(
        input_gate_logits, forget_gate_logits, forget_decay_offset
    )
    cumulative = jnp.cumsum(forget_log_sigmoid, axis=0)
    total_log = cumulative[-1]
    block_count = token_count // BLOCK

    def blocks(tensor):
        return tensor.reshape((block_count, BLOCK) + tensor.shape[1:])

    initial = (
        jnp.zeros((head_count, value_width, key_width), jnp.float32),
        jnp.zeros((head_count, key_width), jnp.float32),
        jnp.full((head_count,), neg_large, jnp.float32),
    )
    end_state, (numerator, denominator, stable) = lax.scan(
        local_step,
        initial,
        (
            blocks(queries_low),
            blocks(keys_low),
            blocks(values_low),
            blocks(input_log_value),
            blocks(forget_log_sigmoid),
        ),
    )
    end_memory, end_normer, end_running = end_state
    identity = (
        jnp.zeros((head_count,), jnp.float32),
        jnp.zeros((head_count, value_width, key_width), jnp.float32),
        jnp.zeros((head_count, key_width), jnp.float32),
        jnp.full((head_count,), neg_large, jnp.float32),
    )
    prefix = carried_in(
        (total_log, end_memory, end_normer, end_running), "sp", combine_states, identity
    )
    numerator = numerator.reshape(token_count, head_count, value_width)
    denominator = denominator.reshape(token_count, head_count)
    stable = stable.reshape(token_count, head_count)
    _, prior_memory, prior_normer, prior_running = prefix
    scaled_query = queries_low.astype(jnp.float32) * query_scale
    prior_log = cumulative + prior_running[None, :]
    top_log = jnp.maximum(stable, prior_log)
    local_weight = jnp.exp(stable - top_log)
    prior_weight = jnp.exp(prior_log - top_log)
    numerator = local_weight[:, :, None] * numerator + prior_weight[:, :, None] * jnp.einsum(
        "hvd,thd->thv", prior_memory, scaled_query, precision=highest
    )
    denominator = local_weight * denominator + prior_weight * jnp.einsum(
        "hd,thd->th", prior_normer, scaled_query, precision=highest
    )
    memory_out = numerator / jnp.maximum(jnp.abs(denominator), jnp.exp(-top_log))[:, :, None]
    normed = (
        memory_out
        * lax.rsqrt(jnp.mean(memory_out * memory_out, axis=-1, keepdims=True) + eps)
        * head_norm_gain[None, :, :]
    )
    gated_rows = (
        normed.reshape(token_count, head_count * value_width)
        * jax.nn.sigmoid(output_gate_logits.astype(jnp.float32))
    ).astype(jnp.bfloat16)
    whole_out = lax.all_gather(cell_output_weight, "tp", axis=0, tiled=True)
    own_rows = lax.all_to_all(gated_rows, "tp", split_axis=0, concat_axis=1, tiled=True)
    mixed_rows = jnp.dot(own_rows, whole_out, preferred_element_type=jnp.float32)
    stream_wide = residual_entry_input.astype(jnp.float32) + mixed_rows
    stream = stream_wide.astype(jnp.bfloat16)
    stream_wide = lax.optimization_barrier(stream).astype(jnp.float32)
    normed_rows = (
        stream_wide
        * lax.rsqrt(jnp.mean(stream_wide * stream_wide, axis=-1, keepdims=True) + eps)
        * feedforward_norm_gain[None, :]
    ).astype(jnp.bfloat16)
    group_rows = lax.all_gather(normed_rows, "tp", axis=0, tiled=True)
    earlier_rows = shifted(group_rows[-2:], "sp", 1)
    window = jnp.concatenate([earlier_rows, group_rows], axis=0)
    up_gate = jnp.dot(
        window,
        lax.all_gather(gate_up_weight, "sp", axis=0, tiled=True),
        preferred_element_type=jnp.float32,
    )
    up_value = jnp.dot(
        window,
        lax.all_gather(value_up_weight, "sp", axis=0, tiled=True),
        preferred_element_type=jnp.float32,
    )
    conv_g = (
        gate_filter_taps[0][None, :] * up_gate[:-2]
        + gate_filter_taps[1][None, :] * up_gate[1:-1]
        + gate_filter_taps[2][None, :] * up_gate[2:]
    )
    conv_v = (
        value_filter_taps[0][None, :] * up_value[:-2]
        + value_filter_taps[1][None, :] * up_value[1:-1]
        + value_filter_taps[2][None, :] * up_value[2:]
    )
    hidden = (jax.nn.silu(conv_g) * conv_v).astype(jnp.bfloat16)
    whole_down = lax.all_gather(down_projection_weight, "sp", axis=1, tiled=True)
    ffn_rows = lax.psum_scatter(
        jnp.dot(hidden, whole_down, preferred_element_type=jnp.float32).astype(jnp.bfloat16),
        "tp",
        scatter_dimension=0,
        tiled=True,
    ).astype(jnp.float32)
    return (stream_wide + ffn_rows).astype(jnp.bfloat16)


def solution(mesh):
    in_specs = (
        P(("sp", "tp"), None),
        P("sp", "tp"),
        P("sp", "tp"),
        P("sp", "tp"),
        P("sp", "tp"),
        P("sp", "tp"),
        P("sp", "tp"),
        P("sp", "tp"),
        P("tp", None),
        P("tp", None),
        P(),
        P("sp", "tp"),
        P("sp", "tp"),
        P(None, "tp"),
        P(None, "tp"),
        P("tp", "sp"),
    )
    out_specs = P(("sp", "tp"), None)
    return jax.shard_map(local, mesh=mesh, in_specs=in_specs, out_specs=out_specs, check_vma=False)
```

profile of v0, /device:TPU:0, one launch (start us, length us, event | category | flops | bytes accessed | tf_op | source)
XLA Modules:
  0.0 629.0 jit_solution(18224603662122398015)
XLA Ops:
  12.8 105.2 %while.39 = (s32[]{:T(128)}, f32[2,256,128]{2,1,0:T(8,128)S(1)}, f32[2,128]{1,0:T(2,128)S(1)}, f32[2]{0:T(128)S(1)}, f32[8,128,2,256]{1,0,3,2:T(8,128)}, /*index...) while((s32[]{:T(128)}, f32[2,256,128]{2,1,0:T(8,128)S(1)}, ...), condition=%wide.region_6.7_spmd.clone, body=%wide.region_0.6_spmd.clone.sunk | while | flops 144166400 | bytes 4685610 | solution.py:144
  17.3 8.2 %dynamic_update_slice.19 = f32[8,128,2,256]{1,0,3,2:T(8,128)} dynamic-update-slice(f32[8,128,2,256]{1,0,3,2:T(8,128)} %get-tuple-element.661, f32[1,128,2,256]{1,0,3,2:T(1,128)S(1)} %copy.248, s32[]{:T(128)} %get-tuple-element.657, s32[]{:T(128)} %constant.83.clone.1..sunk, s32[]{:T(128)} %constant.83.clone.1..sunk, s32[]{:T(128)} %constant.83.clone.1..sunk) | dynamic-update-slice | bytes 524292 | tf_op jit(solution)/shard_map/while/body/jit(dynamic_update_index_in_dim)/dynamic_update_slice | solution.py:144
  30.5 8.2 %dynamic_update_slice.19 = f32[8,128,2,256]{1,0,3,2:T(8,128)} dynamic-update-slice(f32[8,128,2,256]{1,0,3,2:T(8,128)} %get-tuple-element.661, f32[1,128,2,256]{1,0,3,2:T(1,128)S(1)} %copy.248, s32[]{:T(128)} %get-tuple-element.657, s32[]{:T(128)} %constant.83.clone.1..sunk, s32[]{:T(128)} %constant.83.clone.1..sunk, s32[]{:T(128)} %constant.83.clone.1..sunk) | dynamic-update-slice | bytes 524292 | tf_op jit(solution)/shard_map/while/body/jit(dynamic_update_index_in_dim)/dynamic_update_slice | solution.py:144
  43.7 8.2 %dynamic_update_slice.19 = f32[8,128,2,256]{1,0,3,2:T(8,128)} dynamic-update-slice(f32[8,128,2,256]{1,0,3,2:T(8,128)} %get-tuple-element.661, f32[1,128,2,256]{1,0,3,2:T(1,128)S(1)} %copy.248, s32[]{:T(128)} %get-tuple-element.657, s32[]{:T(128)} %constant.83.clone.1..sunk, s32[]{:T(128)} %constant.83.clone.1..sunk, s32[]{:T(128)} %constant.83.clone.1..sunk) | dynamic-update-slice | bytes 524292 | tf_op jit(solution)/shard_map/while/body/jit(dynamic_update_index_in_dim)/dynamic_update_slice | solution.py:144
  56.8 8.2 %dynamic_update_slice.19 = f32[8,128,2,256]{1,0,3,2:T(8,128)} dynamic-update-slice(f32[8,128,2,256]{1,0,3,2:T(8,128)} %get-tuple-element.661, f32[1,128,2,256]{1,0,3,2:T(1,128)S(1)} %copy.248, s32[]{:T(128)} %get-tuple-element.657, s32[]{:T(128)} %constant.83.clone.1..sunk, s32[]{:T(128)} %constant.83.clone.1..sunk, s32[]{:T(128)} %constant.83.clone.1..sunk) | dynamic-update-slice | bytes 524292 | tf_op jit(solution)/shard_map/while/body/jit(dynamic_update_index_in_dim)/dynamic_update_slice | solution.py:144
  70.0 8.2 %dynamic_update_slice.19 = f32[8,128,2,256]{1,0,3,2:T(8,128)} dynamic-update-slice(f32[8,128,2,256]{1,0,3,2:T(8,128)} %get-tuple-element.661, f32[1,128,2,256]{1,0,3,2:T(1,128)S(1)} %copy.248, s32[]{:T(128)} %get-tuple-element.657, s32[]{:T(128)} %constant.83.clone.1..sunk, s32[]{:T(128)} %constant.83.clone.1..sunk, s32[]{:T(128)} %constant.83.clone.1..sunk) | dynamic-update-slice | bytes 524292 | tf_op jit(solution)/shard_map/while/body/jit(dynamic_update_index_in_dim)/dynamic_update_slice | solution.py:144
  83.1 8.2 %dynamic_update_slice.19 = f32[8,128,2,256]{1,0,3,2:T(8,128)} dynamic-update-slice(f32[8,128,2,256]{1,0,3,2:T(8,128)} %get-tuple-element.661, f32[1,128,2,256]{1,0,3,2:T(1,128)S(1)} %copy.248, s32[]{:T(128)} %get-tuple-element.657, s32[]{:T(128)} %constant.83.clone.1..sunk, s32[]{:T(128)} %constant.83.clone.1..sunk, s32[]{:T(128)} %constant.83.clone.1..sunk) | dynamic-update-slice | bytes 524292 | tf_op jit(solution)/shard_map/while/body/jit(dynamic_update_index_in_dim)/dynamic_update_slice | solution.py:144
  96.3 8.2 %dynamic_update_slice.19 = f32[8,128,2,256]{1,0,3,2:T(8,128)} dynamic-update-slice(f32[8,128,2,256]{1,0,3,2:T(8,128)} %get-tuple-element.661, f32[1,128,2,256]{1,0,3,2:T(1,128)S(1)} %copy.248, s32[]{:T(128)} %get-tuple-element.657, s32[]{:T(128)} %constant.83.clone.1..sunk, s32[]{:T(128)} %constant.83.clone.1..sunk, s32[]{:T(128)} %constant.83.clone.1..sunk) | dynamic-update-slice | bytes 524292 | tf_op jit(solution)/shard_map/while/body/jit(dynamic_update_index_in_dim)/dynamic_update_slice | solution.py:144
  109.4 8.2 %dynamic_update_slice.19 = f32[8,128,2,256]{1,0,3,2:T(8,128)} dynamic-update-slice(f32[8,128,2,256]{1,0,3,2:T(8,128)} %get-tuple-element.661, f32[1,128,2,256]{1,0,3,2:T(1,128)S(1)} %copy.248, s32[]{:T(128)} %get-tuple-element.657, s32[]{:T(128)} %constant.83.clone.1..sunk, s32[]{:T(128)} %constant.83.clone.1..sunk, s32[]{:T(128)} %constant.83.clone.1..sunk) | dynamic-update-slice | bytes 524292 | tf_op jit(solution)/shard_map/while/body/jit(dynamic_update_index_in_dim)/dynamic_update_slice | solution.py:144
  122.2 22.3 %all-gather.3 = bf16[8,1,2]{2,1,0:T(2,128)(2,1)S(1)} all-gather(bf16[1,1,2]{2,1,0:T(2,128)(2,1)S(1)} %bitcast.273), channel_id=1, replica_groups=mesh['sp'=8,'tp'=4] {'sp'}, dimensions={0}, use_global_device_ids=true | all-gather | bytes 36 | tf_op jit(solution)/shard_map/all_gather | solution.py:14
  144.5 17.5 %all-reduce = bf16[16]{0:T(256)(128)(2,1)S(1)} all-reduce(bf16[16]{0:T(256)(128)(2,1)S(1)} %dynamic-update-slice), channel_id=2, replica_groups=mesh['sp'=8,'tp'=4] {'sp'}, use_global_device_ids=true, to_apply=%add | all-reduce | flops 16 | bytes 64
  166.5 18.0 %all-gather.4 = bf16[8,2,128]{2,1,0:T(2,128)(2,1)S(1)} all-gather(bf16[1,2,128]{2,1,0:T(2,128)(2,1)S(1)} %convert_bitcast_fusion), channel_id=4, replica_groups=mesh['sp'=8,'tp'=4] {'sp'}, dimensions={0}, use_global_device_ids=true | all-gather | bytes 4608 | tf_op jit(solution)/shard_map/all_gather | solution.py:14
  184.5 10.5 %while.40 = (s32[]{:T(128)}, f32[2,256,128]{2,1,0:T(8,128)S(1)}, f32[2,128]{1,0:T(2,128)S(1)}, f32[2]{0:T(128)S(1)}, s32[]{:T(128)}, /*index=5*/bf16[8,2]{0,1:T(...) while((s32[]{:T(128)}, f32[2,256,128]{2,1,0:T(8,128)S(1)}, ...), condition=%wide.region_10.11_spmd.clone, body=%wide.region_9.10_spmd.clone.sunk | while | flops 394772 | bytes 658157 | solution.py:29
  203.1 26.9 %all_to_all.19 = bf16[4,256,512]{2,1,0:T(8,128)(2,1)S(1)} all-to-all(bf16[4,256,512]{2,1,0:T(8,128)(2,1)S(1)} %bitcast.262), channel_id=1, replica_groups=mesh['sp'=8,'tp'=4] {'tp'}, dimensions={0} | all-to-all | bytes 2097152 | tf_op jit(solution)/shard_map/all_to_all | solution.py:191
  230.5 5.7 fusion.45
  239.9 33.9 %all-gather.14.cloned.1.call-done = bf16[1024,2048]{1,0:T(8,128)(2,1)} async-done(((bf16[256,2048]{1,0:T(8,128)(2,1)}), bf16[1024,2048]{1,0:T(8,128)(2,1)}) %all-gather.14.cloned.1.call-update) | async-done | bytes 4194320 | tf_op jit(solution)/shard_map/all_gather | solution.py:201
  274.6 3.4 collective-permute-start
  278.1 90.1 %all-gather.16.cloned.1.call-done = bf16[2048,1408]{1,0:T(8,128)(2,1)} async-done(((bf16[256,1408]{1,0:T(8,128)(2,1)}), bf16[2048,1408]{1,0:T(8,128)(2,1)}) %all-gather.16.cloned.1.call-update) | async-done | bytes 5767184 | tf_op jit(solution)/shard_map/all_gather | solution.py:206
  368.2 11.9 %fusion.44 = f32[1026,1408]{1,0:T(8,128)} fusion(bf16[2048,1408]{1,0:T(8,128)(2,1)} %all-gather.16.cloned.1.call-done, bf16[1024,2048]{1,0:T(8,128)(2,1)} %all-gather.14.cloned.1.call-done, bf16[2,2048]{1,0:T(2,128)(2,1)S(1)} %collective-permute-done), kind=kOutput, calls=%fused_computation.90 | convolution fusion | flops 5925519360 | bytes 15748096 | tf_op jit(solution)/shard_map/dot_general | solution.py:204
  380.1 80.6 %all-gather.18.cloned.1.call-done = bf16[2048,1408]{1,0:T(8,128)(2,1)} async-done(((bf16[256,1408]{1,0:T(8,128)(2,1)}), bf16[2048,1408]{1,0:T(8,128)(2,1)}) %all-gather.18.cloned.1.call-update) | async-done | bytes 5767184 | tf_op jit(solution)/shard_map/all_gather | solution.py:211
  460.7 11.9 %fusion.43 = f32[1026,1408]{1,0:T(8,128)} fusion(bf16[2048,1408]{1,0:T(8,128)(2,1)} %all-gather.18.cloned.1.call-done, bf16[1024,2048]{1,0:T(8,128)(2,1)} %all-gather.14.cloned.1.call-done, bf16[2,2048]{1,0:T(2,128)(2,1)S(1)} %collective-permute-done), kind=kOutput, calls=%fused_computation.89 | convolution fusion | flops 5925519360 | bytes 15748096 | tf_op jit(solution)/shard_map/dot_general | solution.py:209
  472.6 81.3 %all-gather.20.cloned.1.call-done = bf16[1408,2048]{1,0:T(8,128)(2,1)} async-done(((bf16[1408,256]{1,0:T(8,128)(2,1)}), bf16[1408,2048]{1,0:T(8,128)(2,1)}) %all-gather.20.cloned.1.call-update) | async-done | bytes 5767184 | tf_op jit(solution)/shard_map/all_gather | solution.py:225
  554.0 22.7 %convolution_convert_fusion = bf16[1024,2048]{1,0:T(8,128)(2,1)} fusion(bf16[1408,2048]{1,0:T(8,128)(2,1)} %all-gather.20.cloned.1.call-done, f32[1026,1408]{1,0:T(8,128)} %fusion.43, f32[1026,1408]{1,0:T(8,128)} %fusion.44, f32[1408]{0:T(1024)S(1)} %get-tuple-element.403, f32[1408]{0:T(1024)S(1)} %get-tuple-element.404, f32[1408]{0:T(1024)S(1)} %get-tuple-element.402, ...), kind=kOutput, calls=%fused_computation.85 | convolution fusion | flops 5930745856 | bytes 44598272 | tf_op jit(solution)/shard_map/dot_general | solution.py:227
  576.7 42.9 %reduce-scatter.2.cloned.1.call-done = bf16[256,2048]{1,0:T(8,128)(2,1)} async-done(((bf16[1024,2048]{1,0:T(8,128)(2,1)}), bf16[256,2048]{1,0:T(8,128)(2,1)}) %reduce-scatter.2.cloned.1.call-update) | async-done | bytes 1048592 | tf_op jit(solution)/shard_map/reduce_scatter | solution.py:226
  (345 shorter events, 78.8 us)
Async XLA Ops:
  6.5 5.3 copy-start.1
  6.5 178.0 %all-gather.22.cloned.1.call-start = ((), (), s32[]{:S(2)}) async-start(), calls=%async_computation.8 | async-start | bytes 1179648 | tf_op jit(solution)/shard_map/all_gather | solution.py:14
  12.8 107.7 %copy-start.7 = (u32[32]{0:T(128)S(1)}, u32[32]{0:T(128)}, u32[]{:S(2)}) copy-start(u32[32]{0:T(128)} %constant.101) | copy-start | bytes 388
  118.7 111.8 %all-gather.12.cloned.1.call-start = ((), (), s32[]{:S(2)}) async-start(), calls=%async_computation.2 | async-start | bytes 10485760 | tf_op jit(solution)/shard_map/all_gather | solution.py:190
  119.4 154.4 %all-gather.14.cloned.1.call-start = ((), (), s32[]{:S(2)}) async-start(), calls=%async_computation.3 | async-start | bytes 5242880 | tf_op jit(solution)/shard_map/all_gather | solution.py:201
  163.5 31.6 %copy-start.2 = (bf16[1024,256]{1,0:T(8,128)(2,1)S(1)}, bf16[1024,256]{1,0:T(8,128)(2,1)}, u32[]{:S(2)}) copy-start(bf16[1024,256]{1,0:T(8,128)(2,1)} %param.21) | copy-start | bytes 1572868
  196.2 2.3 copy-start.6
  200.6 29.9 %copy-start = (bf16[256,2048]{1,0:T(8,128)(2,1)S(1)}, bf16[256,2048]{1,0:T(8,128)(2,1)}, u32[]{:S(2)}) copy-start(bf16[256,2048]{1,0:T(8,128)(2,1)} %param.20) | copy-start | bytes 3145732
  230.5 6.1 copy-start.5
  236.3 41.7 %copy-start.3 = (f32[3,1408]{1,0:T(4,128)S(1)}, f32[3,1408]{1,0:T(4,128)}, u32[]{:S(2)}) copy-start(f32[3,1408]{1,0:T(4,128)} %param.34) | copy-start | bytes 50692
  236.3 41.7 %copy-start.4 = (f32[3,1408]{1,0:T(4,128)S(1)}, f32[3,1408]{1,0:T(4,128)}, u32[]{:S(2)}) copy-start(f32[3,1408]{1,0:T(4,128)} %param.33) | copy-start | bytes 50692
  237.9 130.3 %all-gather.16.cloned.1.call-start = ((), (), s32[]{:S(2)}) async-start(), calls=%async_computation.4 | async-start | bytes 6488064 | tf_op jit(solution)/shard_map/all_gather | solution.py:206
  238.5 222.3 %all-gather.18.cloned.1.call-start = ((), (), s32[]{:S(2)}) async-start(), calls=%async_computation.5 | async-start | bytes 6488064 | tf_op jit(solution)/shard_map/all_gather | solution.py:211
  239.1 314.9 %all-gather.20.cloned.1.call-start = ((), (), s32[]{:S(2)}) async-start(), calls=%async_computation.6 | async-start | bytes 6488064 | tf_op jit(solution)/shard_map/all_gather | solution.py:225
  239.7 379.9 %reduce-scatter.2.cloned.1.call-start = ((), (), s32[]{:S(2)}) async-start(), calls=%async_computation.7 | async-start | bytes 5242880 | tf_op jit(solution)/shard_map/reduce_scatter | solution.py:226
  274.6 93.6 %collective-permute-start = (bf16[2,2048]{1,0:T(2,128)(2,1)S(1)}, bf16[2,2048]{1,0:T(2,128)(2,1)S(1)}, u32[]{:S(2)}, u32[]{:S(2)}) collective-permute-start(bf16[2,2048]{1,0:T(2,128)(2,1)S(1)} %slice.72), channel_id=1, source_target_pairs={{0,4},{4,8},{8,12},{12,16},{16,20},{20,24},{24,28},{1,5},{5,9},{9,... | collective-permute-start | bytes 24584 | tf_op jit(solution)/shard_map/ppermute | solution.py:35
Sparse Core Ops, SparseCore 0:
  118.8 43.2 all-gather.21
  163.6 66.6 all-gather.11
  238.0 35.7 all-gather.13
  275.8 92.3 all-gather.15
  370.2 90.4 all-gather.17
  462.6 91.2 all-gather.19
  576.8 42.7 reduce-scatter.1
where the time goes:
time: 631 us; the launch traced here: 629 us
  waiting for transfers between devices  331 us (52%)
  local copies, waits for them, and re-layouts  97.1 us (15%)
  blocking collectives  84.7 us (13%)
  matrix products  67.5 us (11%)
  other arithmetic  29.4 us (5%)
  between operations  14.4 us (2%)
    all_gather x1, waiting for transfers between devices, local(): lax.all_gather(gate_up_weight, 'sp', axis=0, tiled=True)  90.1 us
    all_gather x1, waiting for transfers between devices, local(): lax.all_gather(down_projection_weight, 'sp', axis=1, tiled=True)  81.3 us
    all_gather x1, waiting for transfers between devices, local(): lax.all_gather(value_up_weight, 'sp', axis=0, tiled=True)  80.6 us
    dynamic_update_slice x16, local copies, waits for them, and re-layouts, local(): lax.scan(local_step, initial, (blocks(queries_low), blocks(keys_low), blo...  66.7 us
    reduce_scatter x1, waiting for transfers between devices, local(): lax.psum_scatter(jnp.dot(hidden, whole_down, preferred_element_type=jnp.f...  42.9 us
    all_gather x2, blocking collectives, carried_in(): lax.all_gather(part.astype(kind), axis)  40.3 us
    all_gather x1, waiting for transfers between devices, local(): group_rows = lax.all_gather(normed_rows, 'tp', axis=0, tiled=True)  33.9 us
    all_to_all x1, blocking collectives, local(): lax.all_to_all(gated_rows, 'tp', split_axis=0, concat_axis=1, tiled=True)  26.9 us
  transfers between devices with their start and end apart: 8, of which 5 were waited for; matrix products, arithmetic and copies ran while one was open for 8% of the time, Pallas kernels for 0%

commit v1 on v0

--- a/solution.py
+++ b/solution.py
@@ -6,6 +6,22 @@
 BLOCK = 128
 eps = 1e-06
 neg_large = -1e30
+
+
+def _expand_chunk(vec, mesh_dim):
+    inbox = [vec]
+    n_shards = lax.axis_size(mesh_dim)
+    for to_i in range(n_shards - 1):
+        inbox.append(
+            lax.ppermute(
+                inbox[-1],
+                axis_name=mesh_dim,
+                perm=[(pp, (pp + 1) % n_shards) for pp in range(n_shards)],
+            )
+        )
+    r_now = jnp.concatenate(inbox[::-1], axis=1)
+    wide_out = jnp.roll(r_now, (lax.axis_index(mesh_dim) + 1) * vec.shape[1], axis=1)
+    return wide_out
 
 
 def carried_in(x, axis, combine, identity):
@@ -222,7 +238,7 @@
         + value_filter_taps[2][None, :] * up_value[2:]
     )
     hidden = (jax.nn.silu(conv_g) * conv_v).astype(jnp.bfloat16)
-    whole_down = lax.all_gather(down_projection_weight, "sp", axis=1, tiled=True)
+    whole_down = _expand_chunk(down_projection_weight, "sp")
     ffn_rows = lax.psum_scatter(
         jnp.dot(hidden, whole_down, preferred_element_type=jnp.float32).astype(jnp.bfloat16),
         "tp",

time: 631 us -> 604 us (0.957)
  waiting for transfers between devices: 331 us -> 277 us
  local copies, waits for them, and re-layouts: 97.1 us -> 123 us
    ppermute x0 -> x7, waiting for transfers between devices: none -> 188 us  [_expand_chunk(): lax.ppermute(inbox[-1], axis_name=mesh_dim, perm=[(pp, (pp + 1) % n_shard...]
    all_gather x1 -> x0, waiting for transfers between devices: 81.3 us -> none  [local(): lax.all_gather(down_projection_weight, 'sp', axis=1, tiled=True)]
    all_gather x1, waiting for transfers between devices: 80.6 us -> 0.01 us  [local(): lax.all_gather(value_up_weight, 'sp', axis=0, tiled=True)]
    all_gather x1, waiting for transfers between devices: 90.1 us -> 43.6 us  [local(): lax.all_gather(gate_up_weight, 'sp', axis=0, tiled=True)]
    all_gather x1, waiting for transfers between devices: 33.9 us -> 0.01 us  [local(): group_rows = lax.all_gather(normed_rows, 'tp', axis=0, tiled=True)]
    unnamed x21 -> x48, local copies, waits for them, and re-layouts: 0.89 us -> 24.9 us
  transfers between devices with their start and end apart: 8 -> 14, of which waited for: 5 -> 11; matrix products, arithmetic and copies ran while one was open for 8% -> 10% of each run, Pallas kernels for 0% -> 0%
where the time goes in v1:
time: 604 us; the launch traced here: 602 us
  waiting for transfers between devices  277 us (46%)
  local copies, waits for them, and re-layouts  123 us (20%)
  blocking collectives  85.1 us (14%)
  matrix products  68.5 us (11%)
  other arithmetic  29.2 us (5%)
  between operations  14.3 us (2%)
    ppermute x7, waiting for transfers between devices, _expand_chunk(): lax.ppermute(inbox[-1], axis_name=mesh_dim, perm=[(pp, (pp + 1) % n_shard...  188 us
    dynamic_update_slice x16, local copies, waits for them, and re-layouts, local(): lax.scan(local_step, initial, (blocks(queries_low), blocks(keys_low), blo...  66.7 us
    all_gather x1, waiting for transfers between devices, local(): lax.all_gather(gate_up_weight, 'sp', axis=0, tiled=True)  43.6 us
    reduce_scatter x1, waiting for transfers between devices, local(): lax.psum_scatter(jnp.dot(hidden, whole_down, preferred_element_type=jnp.f...  42.9 us
    all_gather x2, blocking collectives, carried_in(): lax.all_gather(part.astype(kind), axis)  40.3 us
    all_to_all x1, blocking collectives, local(): lax.all_to_all(gated_rows, 'tp', split_axis=0, concat_axis=1, tiled=True)  27.3 us
    unnamed x48, local copies, waits for them, and re-layouts  24.9 us
    dot_general x1, matrix products, local(): jnp.dot(hidden, whole_down, preferred_element_type=jnp.float32)  23.7 us
  transfers between devices with their start and end apart: 14, of which 11 were waited for; matrix products, arithmetic and copies ran while one was open for 10% of the time, Pallas kernels for 0%

profile of v1, /device:TPU:0, one launch (start us, length us, event | category | flops | bytes accessed | tf_op | source)
XLA Modules:
  0.0 601.8 jit_solution(10842242744348345828)
XLA Ops:
  13.8 105.1 %while.39 = (s32[]{:T(128)}, f32[2,256,128]{2,1,0:T(8,128)S(1)}, f32[2,128]{1,0:T(2,128)S(1)}, f32[2]{0:T(128)S(1)}, f32[8,128,2,256]{1,0,3,2:T(8,128)}, /*index...) while((s32[]{:T(128)}, f32[2,256,128]{2,1,0:T(8,128)S(1)}, ...), condition=%wide.region_6.7_spmd.clone, body=%wide.region_0.6_spmd.clone.sunk | while | flops 144166400 | bytes 4685110 | solution.py:160
  18.7 8.2 %dynamic_update_slice.19 = f32[8,128,2,256]{1,0,3,2:T(8,128)} dynamic-update-slice(f32[8,128,2,256]{1,0,3,2:T(8,128)} %get-tuple-element.661, f32[1,128,2,256]{1,0,3,2:T(1,128)S(1)} %copy.248, s32[]{:T(128)S(6)} %copy.260, s32[]{:T(128)} %constant.103.clone.1..sunk, s32[]{:T(128)} %constant.103.clone.1..sunk, s32[]{:T(128)} %constant.103.clone.1..sunk) | dynamic-update-slice | bytes 524292 | tf_op jit(solution)/shard_map/while/body/jit(dynamic_update_index_in_dim)/dynamic_update_slice | solution.py:160
  31.8 8.2 %dynamic_update_slice.19 = f32[8,128,2,256]{1,0,3,2:T(8,128)} dynamic-update-slice(f32[8,128,2,256]{1,0,3,2:T(8,128)} %get-tuple-element.661, f32[1,128,2,256]{1,0,3,2:T(1,128)S(1)} %copy.248, s32[]{:T(128)S(6)} %copy.260, s32[]{:T(128)} %constant.103.clone.1..sunk, s32[]{:T(128)} %constant.103.clone.1..sunk, s32[]{:T(128)} %constant.103.clone.1..sunk) | dynamic-update-slice | bytes 524292 | tf_op jit(solution)/shard_map/while/body/jit(dynamic_update_index_in_dim)/dynamic_update_slice | solution.py:160
  45.0 8.2 %dynamic_update_slice.19 = f32[8,128,2,256]{1,0,3,2:T(8,128)} dynamic-update-slice(f32[8,128,2,256]{1,0,3,2:T(8,128)} %get-tuple-element.661, f32[1,128,2,256]{1,0,3,2:T(1,128)S(1)} %copy.248, s32[]{:T(128)S(6)} %copy.260, s32[]{:T(128)} %constant.103.clone.1..sunk, s32[]{:T(128)} %constant.103.clone.1..sunk, s32[]{:T(128)} %constant.103.clone.1..sunk) | dynamic-update-slice | bytes 524292 | tf_op jit(solution)/shard_map/while/body/jit(dynamic_update_index_in_dim)/dynamic_update_slice | solution.py:160
  58.1 8.2 %dynamic_update_slice.19 = f32[8,128,2,256]{1,0,3,2:T(8,128)} dynamic-update-slice(f32[8,128,2,256]{1,0,3,2:T(8,128)} %get-tuple-element.661, f32[1,128,2,256]{1,0,3,2:T(1,128)S(1)} %copy.248, s32[]{:T(128)S(6)} %copy.260, s32[]{:T(128)} %constant.103.clone.1..sunk, s32[]{:T(128)} %constant.103.clone.1..sunk, s32[]{:T(128)} %constant.103.clone.1..sunk) | dynamic-update-slice | bytes 524292 | tf_op jit(solution)/shard_map/while/body/jit(dynamic_update_index_in_dim)/dynamic_update_slice | solution.py:160
  71.3 8.2 %dynamic_update_slice.19 = f32[8,128,2,256]{1,0,3,2:T(8,128)} dynamic-update-slice(f32[8,128,2,256]{1,0,3,2:T(8,128)} %get-tuple-element.661, f32[1,128,2,256]{1,0,3,2:T(1,128)S(1)} %copy.248, s32[]{:T(128)S(6)} %copy.260, s32[]{:T(128)} %constant.103.clone.1..sunk, s32[]{:T(128)} %constant.103.clone.1..sunk, s32[]{:T(128)} %constant.103.clone.1..sunk) | dynamic-update-slice | bytes 524292 | tf_op jit(solution)/shard_map/while/body/jit(dynamic_update_index_in_dim)/dynamic_update_slice | solution.py:160
  97.5 8.2 %dynamic_update_slice.19 = f32[8,128,2,256]{1,0,3,2:T(8,128)} dynamic-update-slice(f32[8,128,2,256]{1,0,3,2:T(8,128)} %get-tuple-element.661, f32[1,128,2,256]{1,0,3,2:T(1,128)S(1)} %copy.248, s32[]{:T(128)S(6)} %copy.260, s32[]{:T(128)} %constant.103.clone.1..sunk, s32[]{:T(128)} %constant.103.clone.1..sunk, s32[]{:T(128)} %constant.103.clone.1..sunk) | dynamic-update-slice | bytes 524292 | tf_op jit(solution)/shard_map/while/body/jit(dynamic_update_index_in_dim)/dynamic_update_slice | solution.py:160
  123.1 22.3 %all-gather.3 = bf16[8,1,2]{2,1,0:T(2,128)(2,1)S(1)} all-gather(bf16[1,1,2]{2,1,0:T(2,128)(2,1)S(1)} %bitcast.274), channel_id=1, replica_groups=mesh['sp'=8,'tp'=4] {'sp'}, dimensions={0}, use_global_device_ids=true | all-gather | bytes 36 | tf_op jit(solution)/shard_map/all_gather | solution.py:30
  145.4 17.5 %all-reduce = bf16[16]{0:T(256)(128)(2,1)S(1)} all-reduce(bf16[16]{0:T(256)(128)(2,1)S(1)} %dynamic-update-slice), channel_id=2, replica_groups=mesh['sp'=8,'tp'=4] {'sp'}, use_global_device_ids=true, to_apply=%add | all-reduce | flops 16 | bytes 64
  167.3 18.0 %all-gather.4 = bf16[8,2,128]{2,1,0:T(2,128)(2,1)S(1)} all-gather(bf16[1,2,128]{2,1,0:T(2,128)(2,1)S(1)} %convert_bitcast_fusion), channel_id=4, replica_groups=mesh['sp'=8,'tp'=4] {'sp'}, dimensions={0}, use_global_device_ids=true | all-gather | bytes 4608 | tf_op jit(solution)/shard_map/all_gather | solution.py:30
  185.4 10.5 %while.40 = (s32[]{:T(128)}, f32[2,256,128]{2,1,0:T(8,128)S(1)}, f32[2,128]{1,0:T(2,128)S(1)}, f32[2]{0:T(128)S(1)}, s32[]{:T(128)}, /*index=5*/bf16[8,2]{0,1:T(...) while((s32[]{:T(128)}, f32[2,256,128]{2,1,0:T(8,128)S(1)}, ...), condition=%wide.region_10.11_spmd.clone, body=%wide.region_9.10_spmd.clone.sunk | while | flops 394772 | bytes 658165 | solution.py:45
  203.6 27.3 %all_to_all.19 = bf16[4,256,512]{2,1,0:T(8,128)(2,1)S(1)} all-to-all(bf16[4,256,512]{2,1,0:T(8,128)(2,1)S(1)} %bitcast.261), channel_id=1, replica_groups=mesh['sp'=8,'tp'=4] {'tp'}, dimensions={0} | all-to-all | bytes 2097152 | tf_op jit(solution)/shard_map/all_to_all | solution.py:207
  242.5 19.3 %collective-permute-done.1 = bf16[1408,256]{1,0:T(8,128)(2,1)S(1)} collective-permute-done((bf16[1408,256]{1,0:T(8,128)(2,1)S(1)}, bf16[1408,256]{1,0:T(8,128)(2,1)S(1)}, u32[]{:S(2)}, u32[]{:S(2)}) %collective-permute-start.1) | collective-permute-done | bytes 720928 | tf_op jit(solution)/shard_map/ppermute | solution.py:16
  261.8 20.3 %collective-permute-done.2 = bf16[1408,256]{1,0:T(8,128)(2,1)S(1)} collective-permute-done((bf16[1408,256]{1,0:T(8,128)(2,1)S(1)}, bf16[1408,256]{1,0:T(8,128)(2,1)S(1)}, u32[]{:S(2)}, u32[]{:S(2)}) %collective-permute-start.2) | collective-permute-done | bytes 720928 | tf_op jit(solution)/shard_map/ppermute | solution.py:16
  282.2 32.6 %collective-permute-done.3 = bf16[1408,256]{1,0:T(8,128)(2,1)S(1)} collective-permute-done((bf16[1408,256]{1,0:T(8,128)(2,1)S(1)}, bf16[1408,256]{1,0:T(8,128)(2,1)S(1)}, u32[]{:S(2)}, u32[]{:S(2)}) %collective-permute-start.3) | collective-permute-done | bytes 720928 | tf_op jit(solution)/shard_map/ppermute | solution.py:16
  315.6 24.8 %collective-permute-done.4 = bf16[1408,256]{1,0:T(8,128)(2,1)S(1)} collective-permute-done((bf16[1408,256]{1,0:T(8,128)(2,1)S(1)}, bf16[1408,256]{1,0:T(8,128)(2,1)S(1)}, u32[]{:S(2)}, u32[]{:S(2)}) %collective-permute-start.4) | collective-permute-done | bytes 720928 | tf_op jit(solution)/shard_map/ppermute | solution.py:16
  341.3 36.1 %collective-permute-done.5 = bf16[1408,256]{1,0:T(8,128)(2,1)S(1)} collective-permute-done((bf16[1408,256]{1,0:T(8,128)(2,1)S(1)}, bf16[1408,256]{1,0:T(8,128)(2,1)S(1)}, u32[]{:S(2)}, u32[]{:S(2)}) %collective-permute-start.5) | collective-permute-done | bytes 720928 | tf_op jit(solution)/shard_map/ppermute | solution.py:16
  378.3 34.1 %collective-permute-done.6 = bf16[1408,256]{1,0:T(8,128)(2,1)} collective-permute-done((bf16[1408,256]{1,0:T(8,128)(2,1)S(1)}, bf16[1408,256]{1,0:T(8,128)(2,1)}, u32[]{:S(2)}, u32[]{:S(2)}) %collective-permute-start.6) | collective-permute-done | bytes 720928 | tf_op jit(solution)/shard_map/ppermute | solution.py:16
  412.5 21.2 %collective-permute-done.7 = bf16[1408,256]{1,0:T(8,128)(2,1)} collective-permute-done((bf16[1408,256]{1,0:T(8,128)(2,1)}, bf16[1408,256]{1,0:T(8,128)(2,1)}, u32[]{:S(2)}, u32[]{:S(2)}) %collective-permute-start.7) | collective-permute-done | bytes 720928 | tf_op jit(solution)/shard_map/ppermute | solution.py:16
  458.6 11.8 %fusion.48 = f32[1026,1408]{1,0:T(8,128)} fusion(bf16[2048,1408]{1,0:T(8,128)(2,1)} %all-gather.17.cloned.1.call-done, bf16[1024,2048]{1,0:T(8,128)(2,1)} %all-gather.13.cloned.1.call-done, bf16[2,2048]{1,0:T(2,128)(2,1)S(1)} %collective-permute-done), kind=kOutput, calls=%fused_computation.91 | convolution fusion | flops 5925519360 | bytes 15748096 | tf_op jit(solution)/shard_map/dot_general | solution.py:225
  470.4 43.6 %all-gather.15.cloned.1.call-done = bf16[2048,1408]{1,0:T(8,128)(2,1)} async-done(((bf16[256,1408]{1,0:T(8,128)(2,1)}), bf16[2048,1408]{1,0:T(8,128)(2,1)}) %all-gather.15.cloned.1.call-update) | async-done | bytes 5767184 | tf_op jit(solution)/shard_map/all_gather | solution.py:222
  513.9 11.8 %fusion.49 = f32[1026,1408]{1,0:T(8,128)} fusion(bf16[2048,1408]{1,0:T(8,128)(2,1)} %all-gather.15.cloned.1.call-done, bf16[1024,2048]{1,0:T(8,128)(2,1)} %all-gather.13.cloned.1.call-done, bf16[2,2048]{1,0:T(2,128)(2,1)S(1)} %collective-permute-done), kind=kOutput, calls=%fused_computation.92 | convolution fusion | flops 5925519360 | bytes 15748096 | tf_op jit(solution)/shard_map/dot_general | solution.py:220
  525.8 23.7 %fusion.44 = bf16[1024,2048]{1,0:T(8,128)(2,1)} fusion(bf16[1408,4096]{1,0:T(8,128)(2,1)} %constant_dynamic-update-slice_fusion, s32[]{:T(128)S(6)} %select_n.82, f32[1026,1408]{1,0:T(8,128)} %fusion.48, f32[1026,1408]{1,0:T(8,128)} %fusion.49, f32[1408]{0:T(1024)S(1)} %get-tuple-element.403, f32[1408]{0:T(1024)S(1)} %get-tuple-element.404, ...), kind=kOutput, calls=%fused_computation.87 | convolution fusion | flops 5930745856 | bytes 44598276 | tf_op jit(solution)/shard_map/dot_general | solution.py:243
  549.5 42.9 %reduce-scatter.2.cloned.1.call-done = bf16[256,2048]{1,0:T(8,128)(2,1)} async-done(((bf16[1024,2048]{1,0:T(8,128)(2,1)}), bf16[256,2048]{1,0:T(8,128)(2,1)}) %reduce-scatter.2.cloned.1.call-update) | async-done | bytes 1048592 | tf_op jit(solution)/shard_map/reduce_scatter | solution.py:242
  (384 shorter events, 130.0 us)
Async XLA Ops:
  6.5 178.8 %all-gather.19.cloned.1.call-start = ((), (), s32[]{:S(2)}) async-start(), calls=%async_computation.7 | async-start | bytes 1179648 | tf_op jit(solution)/shard_map/all_gather | solution.py:30
  13.8 107.7 %copy-start.13 = (u32[32]{0:T(128)S(1)}, u32[32]{0:T(128)}, u32[]{:S(2)}) copy-start(u32[32]{0:T(128)} %constant.126) | copy-start | bytes 388
  118.9 77.0 %copy-start.8 = (bf16[1024,256]{1,0:T(8,128)(2,1)S(1)}, bf16[1024,256]{1,0:T(8,128)(2,1)}, u32[]{:S(2)}) copy-start(bf16[1024,256]{1,0:T(8,128)(2,1)} %param.21) | copy-start | bytes 1572868
  119.6 112.2 %all-gather.11.cloned.1.call-start = ((), (), s32[]{:S(2)}) async-start(), calls=%async_computation.2 | async-start | bytes 10485760 | tf_op jit(solution)/shard_map/all_gather | solution.py:206
  120.3 334.8 %all-gather.13.cloned.1.call-start = ((), (), s32[]{:S(2)}) async-start(), calls=%async_computation.3 | async-start | bytes 5242880 | tf_op jit(solution)/shard_map/all_gather | solution.py:217
  195.9 3.4 copy-start.12
  231.8 6.3 %copy-start.11 = (f32[2048]{0:T(1024)S(1)}, f32[2048]{0:T(1024)}, u32[]{:S(2)}) copy-start(f32[2048]{0:T(1024)} %param.30) | copy-start | bytes 24580
  231.8 8.3 %copy-start = (bf16[1408,256]{1,0:T(8,128)(2,1)S(1)}, bf16[1408,256]{1,0:T(8,128)(2,1)}, u32[]{:S(2)}) copy-start(bf16[1408,256]{1,0:T(8,128)(2,1)} %param.35) | copy-start | bytes 2162692
  231.8 180.6 %copy-start.9 = (f32[3,1408]{1,0:T(4,128)S(1)}, f32[3,1408]{1,0:T(4,128)}, u32[]{:S(2)}) copy-start(f32[3,1408]{1,0:T(4,128)} %param.34) | copy-start | bytes 50692
  231.8 180.6 %copy-start.10 = (f32[3,1408]{1,0:T(4,128)S(1)}, f32[3,1408]{1,0:T(4,128)}, u32[]{:S(2)}) copy-start(f32[3,1408]{1,0:T(4,128)} %param.33) | copy-start | bytes 50692
  239.4 218.8 %all-gather.17.cloned.1.call-start = ((), (), s32[]{:S(2)}) async-start(), calls=%async_computation.5 | async-start | bytes 6488064 | tf_op jit(solution)/shard_map/all_gather | solution.py:227
  240.0 273.9 %all-gather.15.cloned.1.call-start = ((), (), s32[]{:S(2)}) async-start(), calls=%async_computation.4 | async-start | bytes 6488064 | tf_op jit(solution)/shard_map/all_gather | solution.py:222
  240.0 21.7 %collective-permute-start.1 = (bf16[1408,256]{1,0:T(8,128)(2,1)S(1)}, bf16[1408,256]{1,0:T(8,128)(2,1)S(1)}, u32[]{:S(2)}, u32[]{:S(2)}) collective-permute-start(bf16[1408,256]{1,0:T(8,128)(2,1)S(1)} %copy-done), channel_id=1, source_target_pairs={{0,4},{4,8},{8,12},{12,16},{16,20},{20,24},{24,28},{28,0},{1,5},{5... | collective-permute-start | bytes 2162696 | tf_op jit(solution)/shard_map/ppermute | solution.py:16
  261.8 20.4 %collective-permute-start.2 = (bf16[1408,256]{1,0:T(8,128)(2,1)S(1)}, bf16[1408,256]{1,0:T(8,128)(2,1)S(1)}, u32[]{:S(2)}, u32[]{:S(2)}) collective-permute-start(bf16[1408,256]{1,0:T(8,128)(2,1)S(1)} %collective-permute-done.1), channel_id=1, source_target_pairs={{0,4},{4,8},{8,12},{12,16},{16,20},{20,24},{24,28},{28,0},{1,5},{5... | collective-permute-start | bytes 2162696 | tf_op jit(solution)/shard_map/ppermute | solution.py:16
  261.8 330.6 %reduce-scatter.2.cloned.1.call-start = ((), (), s32[]{:S(2)}) async-start(), calls=%async_computation.6 | async-start | bytes 5242880 | tf_op jit(solution)/shard_map/reduce_scatter | solution.py:242
  282.2 32.6 %collective-permute-start.3 = (bf16[1408,256]{1,0:T(8,128)(2,1)S(1)}, bf16[1408,256]{1,0:T(8,128)(2,1)S(1)}, u32[]{:S(2)}, u32[]{:S(2)}) collective-permute-start(bf16[1408,256]{1,0:T(8,128)(2,1)S(1)} %collective-permute-done.2), channel_id=1, source_target_pairs={{0,4},{4,8},{8,12},{12,16},{16,20},{20,24},{24,28},{28,0},{1,5},{5... | collective-permute-start | bytes 2162696 | tf_op jit(solution)/shard_map/ppermute | solution.py:16
  315.6 24.8 %collective-permute-start.4 = (bf16[1408,256]{1,0:T(8,128)(2,1)S(1)}, bf16[1408,256]{1,0:T(8,128)(2,1)S(1)}, u32[]{:S(2)}, u32[]{:S(2)}) collective-permute-start(bf16[1408,256]{1,0:T(8,128)(2,1)S(1)} %collective-permute-done.3), channel_id=1, source_target_pairs={{0,4},{4,8},{8,12},{12,16},{16,20},{20,24},{24,28},{28,0},{1,5},{5... | collective-permute-start | bytes 2162696 | tf_op jit(solution)/shard_map/ppermute | solution.py:16
  341.3 36.1 %collective-permute-start.5 = (bf16[1408,256]{1,0:T(8,128)(2,1)S(1)}, bf16[1408,256]{1,0:T(8,128)(2,1)S(1)}, u32[]{:S(2)}, u32[]{:S(2)}) collective-permute-start(bf16[1408,256]{1,0:T(8,128)(2,1)S(1)} %collective-permute-done.4), channel_id=1, source_target_pairs={{0,4},{4,8},{8,12},{12,16},{16,20},{20,24},{24,28},{28,0},{1,5},{5... | collective-permute-start | bytes 2162696 | tf_op jit(solution)/shard_map/ppermute | solution.py:16
  378.3 34.1 %collective-permute-start.6 = (bf16[1408,256]{1,0:T(8,128)(2,1)S(1)}, bf16[1408,256]{1,0:T(8,128)(2,1)}, u32[]{:S(2)}, u32[]{:S(2)}) collective-permute-start(bf16[1408,256]{1,0:T(8,128)(2,1)S(1)} %collective-permute-done.5), channel_id=1, source_target_pairs={{0,4},{4,8},{8,12},{12,16},{16,20},{20,24},{24,28},{28,0},{1,5},{5... | collective-permute-start | bytes 2162696 | tf_op jit(solution)/shard_map/ppermute | solution.py:16
  412.4 21.3 %collective-permute-start.7 = (bf16[1408,256]{1,0:T(8,128)(2,1)}, bf16[1408,256]{1,0:T(8,128)(2,1)}, u32[]{:S(2)}, u32[]{:S(2)}) collective-permute-start(bf16[1408,256]{1,0:T(8,128)(2,1)} %collective-permute-done.6), channel_id=1, source_target_pairs={{0,4},{4,8},{8,12},{12,16},{16,20},{20,24},{24,28},{28,0},{1,5},{5... | collective-permute-start | bytes 2162696 | tf_op jit(solution)/shard_map/ppermute | solution.py:16
  412.4 29.9 %copy-start.2 = (bf16[1408,256]{1,0:T(8,128)(2,1)S(1)}, bf16[1408,256]{1,0:T(8,128)(2,1)}, u32[]{:S(2)}) copy-start(bf16[1408,256]{1,0:T(8,128)(2,1)} %copy-done.1) | copy-start | bytes 2162692
  437.9 12.4 %copy-start.6 = (bf16[1408,256]{1,0:T(8,128)(2,1)S(1)}, bf16[1408,256]{1,0:T(8,128)(2,1)}, u32[]{:S(2)}) copy-start(bf16[1408,256]{1,0:T(8,128)(2,1)} %copy-done.5) | copy-start | bytes 2162692
  440.1 11.2 %copy-start.4 = (bf16[1408,256]{1,0:T(8,128)(2,1)S(1)}, bf16[1408,256]{1,0:T(8,128)(2,1)}, u32[]{:S(2)}) copy-start(bf16[1408,256]{1,0:T(8,128)(2,1)} %copy-done.3) | copy-start | bytes 2162692
  455.9 2.6 collective-permute-start
  (4 other events, 4.8 us)
Sparse Core Ops, SparseCore 0:
  119.7 43.2 all-gather.18
  164.5 67.1 all-gather.10
  239.5 35.3 all-gather.12
  276.9 133.1 all-gather.16
  412.2 101.6 all-gather.14
  549.6 42.7 reduce-scatter.1
